TPU v7x, 32 devices: a whole 2x2x4 slice. The times are simulated.
32 devices in a mesh: ep: 4 (over y, x), tp: 8 (over z, core).
Axes of the slice: x: 2, y: 2, z: 4, core: 2. Of those that a mesh axis runs over, the one named last changes fastest.
Arguments:
- tokens: bfloat16 [64, 2048], P('ep'), may hold values from -6 to 6
- routes: int32 [64, 4], P('ep'), may hold values from 0 to 7, all different within a row; in each aligned block of 16 rows (0 to 15, 16 to 31, ...) at most 16 rows name the same one
- route_weight: float32 [64, 4], P('ep'), may hold values from 0.2 to 1
- mixer_gain: float32 [2048], replicated, may hold values from 0.1 to 1.9
- gate_weight: bfloat16 [2048, 4096], P(None, 'tp'), may hold values from -0.125 to 0.125
- input_weight: bfloat16 [2048, 4096], P(None, 'tp'), may hold values from -0.125 to 0.125
- step_weight: bfloat16 [2048, 64], P(None, 'tp'), may hold values from -0.125 to 0.125
- write_weight: bfloat16 [2048, 512], P('tp'), may hold values from -0.125 to 0.125
- read_weight: bfloat16 [2048, 512], P('tp'), may hold values from -0.125 to 0.125
- step_bias: float32 [64], P('tp'), may hold values from -3 to 0.5
- decay_log: float32 [64], P('tp'), may hold values from -2 to 0.5
- decay_jolt: float32 [64, 64], P('ep', 'tp'), may hold values from -1 to 0
- filter_taps: bfloat16 [4, 4096], P(None, 'tp'), may hold values from -3 to 3
- filter_state: bfloat16 [64, 3, 4096], P('ep', None, 'tp'), may hold values from -6 to 6
- scan_state: float32 [64, 64, 64, 128], P('ep', 'tp'), may hold values from -2 to 2
- skip_gain: float32 [64], P('tp'), may hold values from 0.5 to 2
- head_gain: float32 [4096], P('tp'), may hold values from 0.1 to 1.9
- output_weight: bfloat16 [4096, 2048], P('tp'), may hold values from -0.09375 to 0.09375
- channel_gain: float32 [2048], replicated, may hold values from 0.1 to 1.9
- expert_gate: bfloat16 [8, 2048, 2048], P('ep', None, 'tp'), may hold values from -0.125 to 0.125
- expert_up: bfloat16 [8, 2048, 2048], P('ep', None, 'tp'), may hold values from -0.125 to 0.125
- expert_down: bfloat16 [8, 2048, 2048], P('ep', 'tp'), may hold values from -0.125 to 0.125
- shared_gate: bfloat16 [2048, 2048], P(None, 'tp'), may hold values from -0.125 to 0.125
- shared_up: bfloat16 [2048, 2048], P(None, 'tp'), may hold values from -0.125 to 0.125
- shared_down: bfloat16 [2048, 2048], P('tp'), may hold values from -0.125 to 0.125
Outputs:
- layer_out: bfloat16 [64, 2048], P('ep', 'tp')
- new_state: float32 [64, 64, 64, 128], P('ep', 'tp')
- new_filter: bfloat16 [64, 3, 4096], P('ep', None, 'tp')
Inputs may be any that keep to these rules, and one draw needn't show every extreme that they name: `routes`: each row names 4 different experts. In each aligned block of 16 rows (the rows of one index of ep) no expert is named by more than 16 rows, a bound that some block reaches.
All inputs are finite; a program needn't handle non-finite values.
Results may differ from a plain program's by a relative error of at most 0.025.
Values may be sent and summed in bfloat16 or wider, within the bound.
A program may use at most 64 MiB of HBM per device.

v0:
```python
import jax
import jax.numpy as jnp
from jax import lax
from jax.sharding import PartitionSpec as P

HEADS = 64
HEAD_DIM = 64
GROUPS = 4
STATE = 128
EPS = 1e-06


def rms_normed(values, scaling):
    mean_square = jnp.mean(values * values, axis=-1, keepdims=True)
    return values * lax.rsqrt(mean_square + EPS) * scaling


def route_targets(route_ids, experts, capacity):
    count_rows, top_picks = route_ids.shape
    flattened = route_ids.reshape(count_rows * top_picks)
    onehot = (flattened[:, None] == jnp.arange(experts, dtype=jnp.int32)[None, :]).astype(jnp.int32)
    before = jnp.cumsum(onehot, axis=0) - onehot
    slot_index = jnp.sum(before * onehot, axis=1)
    return (flattened * capacity + slot_index).reshape(count_rows, top_picks)


def expert_terms(token_rows, expert_gate, expert_up, expert_down):
    gate_part = jnp.einsum(
        "ajcd,jdf->ajcf", token_rows, expert_gate, preferred_element_type=jnp.float32
    )
    up_part = jnp.einsum(
        "ajcd,jdf->ajcf", token_rows, expert_up, preferred_element_type=jnp.float32
    )
    hidden = (jax.nn.silu(gate_part) * up_part).astype(jnp.bfloat16)
    return jnp.einsum("ajcf,jfd->ajcd", hidden, expert_down, preferred_element_type=jnp.float32)


def on_device(
    tokens,
    routes,
    route_weight,
    mixer_gain,
    gate_weight,
    input_weight,
    step_weight,
    write_weight,
    read_weight,
    step_bias,
    decay_log,
    decay_jolt,
    filter_taps,
    filter_state,
    scan_state,
    skip_gain,
    head_gain,
    output_weight,
    channel_gain,
    expert_gate,
    expert_up,
    expert_down,
    shared_gate,
    shared_up,
    shared_down,
):
    seq_rows, model_width = tokens.shape
    tp_count = lax.axis_size("tp")
    tp_index = lax.axis_index("tp")
    ep_count = lax.axis_size("ep")
    col_count = model_width // tp_count
    col_start = tp_index * col_count
    tokens_f = tokens.astype(jnp.float32)
    normed = rms_normed(tokens_f, mixer_gain).astype(jnp.bfloat16)
    feature_rows = write_weight.shape[0]
    own_features = lax.dynamic_slice_in_dim(normed, tp_index * feature_rows, feature_rows, 1)
    write_part = jnp.dot(own_features, write_weight, preferred_element_type=jnp.float32)
    read_part = jnp.dot(own_features, read_weight, preferred_element_type=jnp.float32)
    write_in, read_in = (
        lax.psum(write_part.astype(jnp.bfloat16), "tp").astype(jnp.float32),
        lax.psum(read_part.astype(jnp.bfloat16), "tp").astype(jnp.float32),
    )
    gate_rows = jnp.dot(normed, gate_weight, preferred_element_type=jnp.float32).astype(
        jnp.bfloat16
    )
    input_rows = jnp.dot(normed, input_weight, preferred_element_type=jnp.float32).astype(
        jnp.bfloat16
    )
    step_raw = jnp.dot(normed, step_weight, preferred_element_type=jnp.float32)
    window = jnp.concatenate([filter_state, input_rows[:, None, :]], axis=1)
    filtered = jax.nn.silu(
        jnp.sum(window.astype(jnp.float32) * filter_taps.astype(jnp.float32)[None], axis=1)
    )
    step_size = jax.nn.softplus(step_raw + step_bias)
    log_decay = decay_jolt - jnp.exp(decay_log) * step_size
    heads_here = step_bias.shape[0]
    head_input = filtered.reshape(seq_rows, heads_here, HEAD_DIM)
    group_index = tp_index * heads_here // (HEADS // GROUPS)
    write_vec = jax.nn.silu(lax.dynamic_slice_in_dim(write_in, group_index * STATE, STATE, 1))
    read_vec = jax.nn.silu(lax.dynamic_slice_in_dim(read_in, group_index * STATE, STATE, 1))
    new_state = (
        jnp.exp(log_decay)[:, :, None, None] * scan_state
        + (step_size[:, :, None] * head_input)[:, :, :, None] * write_vec[:, None, None, :]
    )
    readout = jnp.einsum("shpn,sn->shp", new_state, read_vec, precision=lax.Precision.HIGHEST)
    readout = readout + skip_gain[None, :, None] * head_input
    gate_heads = gate_rows.astype(jnp.float32).reshape(seq_rows, heads_here, HEAD_DIM)
    gated = rms_normed(readout * jax.nn.silu(gate_heads), head_gain.reshape(heads_here, HEAD_DIM))
    gated = gated.astype(jnp.bfloat16).reshape(seq_rows, heads_here * HEAD_DIM)
    mixer_part = jnp.dot(gated, output_weight, preferred_element_type=jnp.float32)
    mixed = lax.psum(mixer_part.astype(jnp.bfloat16), "tp")
    resid = (tokens_f + mixed.astype(jnp.float32)).astype(jnp.bfloat16)
    normed_ffn = rms_normed(resid.astype(jnp.float32), channel_gain).astype(jnp.bfloat16)
    resid_own = lax.dynamic_slice_in_dim(resid, col_start, col_count, 1)
    shared_hidden = (
        jax.nn.silu(jnp.dot(normed_ffn, shared_gate, preferred_element_type=jnp.float32))
        * jnp.dot(normed_ffn, shared_up, preferred_element_type=jnp.float32)
    ).astype(jnp.bfloat16)
    shared_part = jnp.dot(shared_hidden, shared_down, preferred_element_type=jnp.float32)
    local_experts = expert_gate.shape[0]
    experts = local_experts * ep_count
    top_picks = routes.shape[1]
    capacity = 2 * seq_rows * top_picks // experts
    targets = route_targets(routes, experts, capacity)
    slot_ids = jnp.arange(experts * capacity, dtype=jnp.int32)
    dispatch = jnp.sum((targets[None, :, :] == slot_ids[:, None, None]).astype(jnp.float32), axis=2)
    send_rows = jnp.dot(
        dispatch.astype(jnp.bfloat16), normed_ffn, preferred_element_type=jnp.float32
    )
    send_rows = send_rows.astype(jnp.bfloat16).reshape(
        ep_count, local_experts, capacity, model_width
    )
    terms = expert_terms(
        lax.all_to_all(send_rows, "ep", split_axis=0, concat_axis=0, tiled=True),
        expert_gate,
        expert_up,
        expert_down,
    )
    routed_parts, shared_sum = (
        lax.psum_scatter(terms.astype(jnp.bfloat16), "tp", scatter_dimension=3, tiled=True).astype(
            jnp.float32
        ),
        lax.psum_scatter(
            shared_part.reshape(1, 1, seq_rows, model_width).astype(jnp.bfloat16),
            "tp",
            scatter_dimension=3,
            tiled=True,
        ).astype(jnp.float32),
    )
    expert_rows = routed_parts.astype(jnp.bfloat16)
    returned = lax.all_to_all(expert_rows, "ep", split_axis=0, concat_axis=0, tiled=True)
    returned = returned.reshape(experts * capacity, col_count).astype(jnp.float32)
    combine = jnp.sum(
        jnp.where(targets[:, :, None] == slot_ids[None, None, :], route_weight[:, :, None], 0.0),
        axis=1,
    )
    routed_sum = jnp.dot(combine, returned, precision=lax.Precision.HIGHEST)
    layer_out = (resid_own.astype(jnp.float32) + shared_sum[0, 0] + routed_sum).astype(jnp.bfloat16)
    return (layer_out, new_state, window[:, 1:, :])


def solution(mesh):
    in_specs = (
        P("ep", None),
        P("ep", None),
        P("ep", None),
        P(),
        P(None, "tp"),
        P(None, "tp"),
        P(None, "tp"),
        P("tp", None),
        P("tp", None),
        P("tp"),
        P("tp"),
        P("ep", "tp"),
        P(None, "tp"),
        P("ep", None, "tp"),
        P("ep", "tp", None, None),
        P("tp"),
        P("tp"),
        P("tp", None),
        P(),
        P("ep", None, "tp"),
        P("ep", None, "tp"),
        P("ep", "tp", None),
        P(None, "tp"),
        P(None, "tp"),
        P("tp", None),
    )
    out_specs = (P("ep", "tp"), P("ep", "tp", None, None), P("ep", None, "tp"))
    return jax.shard_map(
        on_device, mesh=mesh, in_specs=in_specs, out_specs=out_specs, check_vma=False
    )
```

profile of v0, /device:TPU:0, one launch (start us, length us, event | category | flops | bytes accessed | tf_op | source)
XLA Modules:
  0.0 199.6 jit_solution(1012858224445261043)
XLA Ops:
  7.2 0.0 all-reduce.3.cloned.1.call-start
  7.3 1.1 fusion.31
  8.4 0.9 fusion.33
  9.4 2.0 fusion.21
  11.4 0.1 reshape.93
  11.5 0.1 convolution_convert_fusion.6
  11.6 0.2 convolution_convert_fusion.5
  11.8 0.1 subtract_exponential_fusion
  11.9 0.1 copy.59
  12.0 2.0 fusion.22
  14.1 0.1 reduce_sum.69
  14.1 0.1 copy.58
  14.2 0.1 mul.206
  14.3 30.3 %all-reduce = (bf16[16,512]{1,0:T(8,128)(2,1)S(1)}, bf16[16,512]{1,0:T(8,128)(2,1)S(1)}) all-reduce(bf16[16,512]{1,0:T(8,128)(2,1)S(1)} %convolution_convert_fusion.6, bf16[16,512]{1,0:T(8,128)(2,1)S(1)} %convolution_convert_fusion.5), channel_id=1, replica_groups=mesh['ep'=4,'tp'=8] {'tp'}, use_global_device_ids=true, to_apply=%region_2.0 | all-reduce | flops 16384 | bytes 65536 | tf_op jit(solution)/shard_map/psum | solution.py:78
  44.6 0.1 broadcast_multiply_fusion
  44.7 3.1 %multiply_add_fusion = f32[16,8,64,128]{3,2,1,0:T(8,128)S(1)} fusion(f32[16,8,64,128]{3,2,1,0:T(8,128)} %param.39, f32[16,128]{1,0:T(8,128)S(1)} %get-tuple-element.12, f32[16,8,64]{2,1,0:T(8,128)S(1)} %broadcast_multiply_fusion, f32[16,8]{1,0:T(8,128)S(1)} %copy.58), kind=kLoop, calls=%fused_computation | loop fusion | flops 3145728 | bytes 8430080 | tf_op jit(solution)/shard_map/add | solution.py:100
  47.8 9.8 %fusion.68 = f32[16,1,8,64]{3,1,2,0:T(1,128)S(1)} fusion(f32[16,8,64,128]{3,2,1,0:T(8,128)S(1)} %multiply_add_fusion, f32[16,128,1,1]{1,2,3,0:T(1,128)S(1)} %bitcast.72), kind=kOutput, calls=%fused_computation.95 | convolution fusion | flops 12582912 | bytes 4235264 | tf_op jit(solution)/shard_map/shpn,sn->shp/dot_general | solution.py:103
  57.6 0.0 copy-start.2
  57.7 0.2 multiply_reduce_fusion.1
  57.9 0.1 multiply_convert_fusion
  58.0 0.1 reshape.89
  58.1 2.6 %convolution_convert_fusion.3 = bf16[16,2048]{1,0:T(8,128)(2,1)} fusion(bf16[16,512]{1,0:T(8,128)(2,1)S(1)} %reshape.89, bf16[512,2048]{1,0:T(8,128)(2,1)} %param.42), kind=kOutput, calls=%fused_computation.5 | convolution fusion | flops 33587200 | bytes 2179072 | tf_op jit(solution)/shard_map/dot_general | solution.py:108
  60.7 0.0 all-reduce.3.cloned.1.call-update
  60.7 0.0 reduce-scatter.5.cloned.1.call-start
  60.7 0.1 copy.60
  60.8 0.1 eq.20
  60.9 0.1 fusion.42
  61.0 0.1 reduce_window_sum.11
  61.1 0.2 select_reduce_fusion.1
  61.3 0.1 reduce_sum.73
  61.4 0.1 copy.61
  61.5 0.1 convert_reduce_fusion
  61.5 52.3 %all-reduce.3.cloned.1.call-done = bf16[16,2048]{1,0:T(8,128)(2,1)} async-done(((bf16[16,2048]{1,0:T(8,128)(2,1)}), bf16[16,2048]{1,0:T(8,128)(2,1)}) %all-reduce.3.cloned.1.call-update) | async-done | bytes 65552 | tf_op jit(solution)/shard_map/psum | solution.py:109
  113.9 1.0 fusion.28
  114.9 0.3 convolution_convert_fusion.1
  115.2 10.6 %all_to_all.10 = bf16[4,2,16,2048]{3,2,1,0:T(8,128)(2,1)S(1)} all-to-all(bf16[4,2,16,2048]{3,2,1,0:T(8,128)(2,1)S(1)} %bitcast.69), channel_id=1, replica_groups=mesh['ep'=4,'tp'=8] {'ep'}, dimensions={0} | all-to-all | bytes 1048576 | tf_op jit(solution)/shard_map/all_to_all | solution.py:132
  125.8 2.1 %fusion.7 = f32[4,2,16,256]{3,2,0,1:T(8,128)S(1)} fusion(bf16[2,2048,256]{2,1,0:T(8,128)(2,1)} %param.44, bf16[4,2,16,2048]{3,2,1,0:T(8,128)(2,1)S(1)} %all_to_all.10), kind=kOutput, calls=%fused_computation.12 | convolution fusion | flops 134217728 | bytes 2752512 | tf_op jit(solution)/shard_map/ajcd,jdf->ajcf/dot_general | solution.py:28
  127.8 3.3 %fusion = bf16[4,2,16,2048]{3,2,0,1:T(8,128)(2,1)} fusion(bf16[2,256,2048]{2,1,0:T(8,128)(2,1)S(1)} %copy-done, bf16[2,2048,256]{2,1,0:T(8,128)(2,1)} %param.45, bf16[4,2,16,2048]{3,2,1,0:T(8,128)(2,1)S(1)} %all_to_all.10, f32[4,2,16,256]{3,2,0,1:T(8,128)S(1)} %fusion.7), kind=kOutput, calls=%fused_computation.3 | convolution fusion | flops 268894208 | bytes 5373952 | tf_op jit(solution)/shard_map/ajcf,jfd->ajcd/dot_general | solution.py:35
  131.1 0.0 reduce-scatter.3.cloned.1.call-start
  131.2 1.5 fusion.65
  132.7 2.9 %fusion.1 = bf16[1,1,16,2048]{3,2,1,0:T(8,128)(2,1)} fusion(bf16[256,2048]{1,0:T(8,128)(2,1)} %param.49, bf16[2048,256]{1,0:T(8,128)(2,1)} %param.48, f32[16,256]{1,0:T(8,128)S(1)} %fusion.65, bf16[16,2048]{1,0:T(8,128)(2,1)S(1)} %get-tuple-element.6, f32[2048]{0:T(1024)S(1)} %copy-done.6, f32[16]{0:T(128)S(1)} %add_rsqrt_fusion.1), kind=kOutput, calls=%fused_computation.6 | convolution fusion | flops 33742848 | bytes 2252864 | tf_op jit(solution)/shard_map/dot_general | solution.py:117
  135.7 0.1 select_reduce_fusion
  135.8 25.0 %reduce-scatter.5.cloned.1.call-done = bf16[4,2,16,256]{3,2,0,1:T(8,128)(2,1)} async-done(((bf16[4,2,16,2048]{3,2,0,1:T(8,128)(2,1)}), bf16[4,2,16,256]{3,2,0,1:T(8,128)(2,1)}) %reduce-scatter.5.cloned.1.call-update) | async-done | bytes 65552 | tf_op jit(solution)/shard_map/reduce_scatter | solution.py:138
  160.8 1.5 copy.64
  162.2 3.6 %all-to-all-start.1 = ((bf16[4,2,16,256]{3,2,1,0:T(8,128)(2,1)}), bf16[4,2,16,256]{3,2,1,0:T(8,128)(2,1)S(1)}, u32[]{:S(2)}, u32[]{:S(2)}) async-start(bf16[4,2,16,256]{3,2,1,0:T(8,128)(2,1)} %copy.64), calls=%async_computation.3 | async-start | bytes 131072 | tf_op jit(solution)/shard_map/all_to_all | solution.py:149
  165.9 0.6 fusion.41
  166.5 25.2 %reduce-scatter.3.cloned.1.call-done = bf16[1,1,16,256]{3,2,1,0:T(8,128)(2,1)} async-done(((bf16[1,1,16,2048]{3,2,1,0:T(8,128)(2,1)}), bf16[1,1,16,256]{3,2,1,0:T(8,128)(2,1)}) %reduce-scatter.3.cloned.1.call-update) | async-done | bytes 8208 | tf_op jit(solution)/shard_map/reduce_scatter | solution.py:141
  191.7 1.4 fusion.24
  (42 shorter events, 0.2 us)
Async XLA Ops:
  7.2 120.7 %copy-start = (bf16[2,256,2048]{2,1,0:T(8,128)(2,1)S(1)}, bf16[2,256,2048]{2,1,0:T(8,128)(2,1)}, u32[]{:S(2)}) copy-start(bf16[2,256,2048]{2,1,0:T(8,128)(2,1)} %param.46) | copy-start | bytes 6291460
  7.2 4.3 %copy-start.3 = (bf16[256,512]{1,0:T(8,128)(2,1)S(1)}, bf16[256,512]{1,0:T(8,128)(2,1)}, u32[]{:S(2)}) copy-start(bf16[256,512]{1,0:T(8,128)(2,1)} %param.32) | copy-start | bytes 786436
  7.2 4.4 %copy-start.4 = (bf16[256,512]{1,0:T(8,128)(2,1)S(1)}, bf16[256,512]{1,0:T(8,128)(2,1)}, u32[]{:S(2)}) copy-start(bf16[256,512]{1,0:T(8,128)(2,1)} %param.33) | copy-start | bytes 786436
  7.2 4.6 %copy-start.14 = (f32[8]{0:T(128)S(1)}, f32[8]{0:T(128)}, u32[]{:S(2)}) copy-start(f32[8]{0:T(128)} %param.35) | copy-start | bytes 100
  7.2 4.6 %copy-start.13 = (f32[16,8]{0,1:T(8,128)S(1)}, f32[16,8]{0,1:T(8,128)}, u32[]{:S(2)}) copy-start(f32[16,8]{0,1:T(8,128)} %param.36) | copy-start | bytes 1540
  7.2 4.6 %copy-start.15 = (f32[8]{0:T(128)S(1)}, f32[8]{0:T(128)}, u32[]{:S(2)}) copy-start(f32[8]{0:T(128)} %param.34) | copy-start | bytes 100
  7.2 4.6 %copy-start.12 = (bf16[2048,8]{0,1:T(8,128)(2,1)S(1)}, bf16[2048,8]{0,1:T(8,128)(2,1)}, u32[]{:S(2)}) copy-start(bf16[2048,8]{0,1:T(8,128)(2,1)} %param.31) | copy-start | bytes 98308
  7.2 106.6 %all-reduce.3.cloned.1.call-start = ((), (), s32[]{:S(2)}) async-start(), calls=%async_computation.4 | async-start | bytes 131072 | tf_op jit(solution)/shard_map/psum | solution.py:109
  9.4 4.6 %copy-start.8 = (bf16[4,512]{1,0:T(4,128)(2,1)S(1)}, bf16[4,512]{1,0:T(4,128)(2,1)}, u32[]{:S(2)}) copy-start(bf16[4,512]{1,0:T(4,128)(2,1)} %param.37) | copy-start | bytes 12292
  9.4 4.7 %copy-start.5 = (bf16[16,3,512]{2,0,1:T(8,128)(2,1)S(1)}, bf16[16,3,512]{2,0,1:T(8,128)(2,1)}, u32[]{:S(2)}) copy-start(bf16[16,3,512]{2,0,1:T(8,128)(2,1)} %param.38) | copy-start | bytes 147460
  11.4 2.8 %copy-start.9 = (f32[512]{0:T(512)S(1)}, f32[512]{0:T(512)}, u32[]{:S(2)}) copy-start(f32[512]{0:T(512)} %param.41) | copy-start | bytes 6148
  47.8 9.8 %copy-start.1 = (f32[16,8,64,128]{3,2,1,0:T(8,128)}, f32[16,8,64,128]{3,2,1,0:T(8,128)S(1)}, u32[]{:S(2)}) copy-start(f32[16,8,64,128]{3,2,1,0:T(8,128)S(1)} %multiply_add_fusion) | copy-start | bytes 12582916
  47.8 9.9 %copy-start.11 = (f32[8]{0:T(128)S(1)}, f32[8]{0:T(128)}, u32[]{:S(2)}) copy-start(f32[8]{0:T(128)} %param.40) | copy-start | bytes 100
  57.6 3.1 %copy-start.7 = (s32[16,4]{0,1:T(4,128)S(1)}, s32[16,4]{0,1:T(4,128)}, u32[]{:S(2)}) copy-start(s32[16,4]{0,1:T(4,128)} %param.26) | copy-start | bytes 772
  57.6 56.2 %copy-start.2 = (bf16[16,2048]{1,0:T(8,128)(2,1)S(1)}, bf16[16,2048]{1,0:T(8,128)(2,1)}, u32[]{:S(2)}) copy-start(bf16[16,2048]{1,0:T(8,128)(2,1)} %param.25) | copy-start | bytes 196612
  57.7 57.2 %copy-start.6 = (f32[2048]{0:T(1024)S(1)}, f32[2048]{0:T(1024)}, u32[]{:S(2)}) copy-start(f32[2048]{0:T(1024)} %param.43) | copy-start | bytes 24580
  60.7 100.1 %reduce-scatter.5.cloned.1.call-start = ((), (), s32[]{:S(2)}) async-start(), calls=%async_computation.6 | async-start | bytes 589824 | tf_op jit(solution)/shard_map/reduce_scatter | solution.py:138
  131.1 4.6 %copy-start.10 = (f32[16,4]{0,1:T(4,128)S(1)}, f32[16,4]{0,1:T(4,128)}, u32[]{:S(2)}) copy-start(f32[16,4]{0,1:T(4,128)} %param.27) | copy-start | bytes 772
  131.1 60.5 %reduce-scatter.3.cloned.1.call-start = ((), (), s32[]{:S(2)}) async-start(), calls=%async_computation.5 | async-start | bytes 73728 | tf_op jit(solution)/shard_map/reduce_scatter | solution.py:141
  162.2 29.4 %all-to-all-start.1 = ((bf16[4,2,16,256]{3,2,1,0:T(8,128)(2,1)}), bf16[4,2,16,256]{3,2,1,0:T(8,128)(2,1)S(1)}, u32[]{:S(2)}, u32[]{:S(2)}) async-start(bf16[4,2,16,256]{3,2,1,0:T(8,128)(2,1)} %copy.64), calls=%async_computation.3 | async-start | bytes 131072 | tf_op jit(solution)/shard_map/all_to_all | solution.py:149
Sparse Core Ops, SparseCore 0:
  60.8 53.0 all-reduce.2
  131.3 29.4 reduce-scatter.4
  163.0 28.6 reduce-scatter.2
where the time goes:
time: 200 us
  waiting for transfers between devices  103 us (52%)
  blocking collectives  40.9 us (20%)
  matrix products  28.4 us (14%)
  between operations  14 us (7%)
  other arithmetic  7.67 us (4%)
  starting transfers between devices  3.77 us (2%)
  local copies, waits for them, and re-layouts  2.39 us (1%)
    psum x1, waiting for transfers between devices, on_device(): mixed = lax.psum(mixer_part.astype(jnp.bfloat16), 'tp')  52.3 us
    psum x1, blocking collectives, on_device(): lax.psum(write_part.astype(jnp.bfloat16), 'tp').astype(jnp.float32)  30.3 us
    reduce_scatter x1, waiting for transfers between devices, on_device(): lax.psum_scatter(shared_part.reshape(1, 1, seq_rows, model_width).astype(...  25.2 us
    reduce_scatter x1, waiting for transfers between devices, on_device(): lax.psum_scatter(terms.astype(jnp.bfloat16), 'tp', scatter_dimension=3, t...  25 us
    all_to_all x1, blocking collectives, on_device(): lax.all_to_all(send_rows, 'ep', split_axis=0, concat_axis=0, tiled=True)  10.6 us
    dot_general x1, matrix products, on_device(): jnp.einsum('shpn,sn->shp', new_state, read_vec, precision=lax.Precision.H...  9.81 us
  transfers between devices with their start and end apart: 4, of which 3 were waited for; matrix products, arithmetic and copies ran while one was open for 4% of the time, Pallas kernels for 0%

commit v1 on v0

--- a/solution.py
+++ b/solution.py
@@ -62,6 +62,11 @@
     shared_up,
     shared_down,
 ):
+
+    def _make_members_all(page, mesh_ax):
+        view_out = lax.all_gather(page, mesh_ax).sum(axis=0)
+        return view_out
+
     seq_rows, model_width = tokens.shape
     tp_count = lax.axis_size("tp")
     tp_index = lax.axis_index("tp")
@@ -75,7 +80,7 @@
     write_part = jnp.dot(own_features, write_weight, preferred_element_type=jnp.float32)
     read_part = jnp.dot(own_features, read_weight, preferred_element_type=jnp.float32)
     write_in, read_in = (
-        lax.psum(write_part.astype(jnp.bfloat16), "tp").astype(jnp.float32),
+        _make_members_all(write_part.astype(jnp.bfloat16), "tp").astype(jnp.float32),
         lax.psum(read_part.astype(jnp.bfloat16), "tp").astype(jnp.float32),
     )
     gate_rows = jnp.dot(normed, gate_weight, preferred_element_type=jnp.float32).astype(

time: 200 us -> 215 us (1.075)
  blocking collectives: 40.9 us -> 55.4 us
    all_gather x0 -> x1, blocking collectives: none -> 15.7 us  [_make_members_all(): view_out = lax.all_gather(page, mesh_ax).sum(axis=0)]
  transfers between devices with their start and end apart: 4 -> 4, of which waited for: 3 -> 3; matrix products, arithmetic and copies ran while one was open for 4% -> 3% of each run, Pallas kernels for 0% -> 0%
where the time goes in v1:
time: 215 us; the launch traced here: 214 us
  waiting for transfers between devices  103 us (48%)
  blocking collectives  55.4 us (26%)
  matrix products  28.4 us (13%)
  between operations  14.1 us (7%)
  other arithmetic  7.7 us (4%)
  starting transfers between devices  3.63 us (2%)
  local copies, waits for them, and re-layouts  2.39 us (1%)
    psum x1, waiting for transfers between devices, on_device(): mixed = lax.psum(mixer_part.astype(jnp.bfloat16), 'tp')  52.3 us
    psum x1, blocking collectives, on_device(): lax.psum(read_part.astype(jnp.bfloat16), 'tp').astype(jnp.float32)  29 us
    reduce_scatter x1, waiting for transfers between devices, on_device(): lax.psum_scatter(shared_part.reshape(1, 1, seq_rows, model_width).astype(...  25.2 us
    reduce_scatter x1, waiting for transfers between devices, on_device(): lax.psum_scatter(terms.astype(jnp.bfloat16), 'tp', scatter_dimension=3, t...  25.1 us
    all_gather x1, blocking collectives, _make_members_all(): view_out = lax.all_gather(page, mesh_ax).sum(axis=0)  15.7 us
    all_to_all x1, blocking collectives, on_device(): lax.all_to_all(send_rows, 'ep', split_axis=0, concat_axis=0, tiled=True)  10.6 us
    dot_general x1, matrix products, on_device(): jnp.einsum('shpn,sn->shp', new_state, read_vec, precision=lax.Precision.H...  9.81 us
  transfers between devices with their start and end apart: 4, of which 3 were waited for; matrix products, arithmetic and copies ran while one was open for 3% of the time, Pallas kernels for 0%

profile of v1, /device:TPU:0, one launch (start us, length us, event | category | flops | bytes accessed | tf_op | source)
XLA Modules:
  0.0 214.1 jit_solution(4638022242160596109)
XLA Ops:
  7.2 0.0 all-reduce.2.cloned.1.call-start
  7.3 1.1 fusion.31
  8.4 0.9 fusion.33
  9.4 2.0 fusion.21
  11.3 0.1 reshape.93
  11.4 0.1 convolution_convert_fusion.6
  11.6 15.7 %all-gather = bf16[128,512]{1,0:T(8,128)(2,1)S(1)} all-gather(bf16[16,512]{1,0:T(8,128)(2,1)S(1)} %convolution_convert_fusion.6), channel_id=2, replica_groups=mesh['ep'=4,'tp'=8] {'tp'}, dimensions={0}, use_global_device_ids=true | all-gather | bytes 147456 | tf_op jit(solution)/shard_map/all_gather | solution.py:67
  27.3 0.1 subtract_exponential_fusion
  27.5 0.1 copy.59
  27.6 2.0 fusion.22
  29.6 0.1 reduce_sum.81
  29.7 0.1 copy.58
  29.8 0.1 convolution_convert_fusion.5
  29.9 29.0 %psum.14 = bf16[16,512]{1,0:T(8,128)(2,1)S(1)} all-reduce(bf16[16,512]{1,0:T(8,128)(2,1)S(1)} %convolution_convert_fusion.5), channel_id=1, replica_groups=mesh['ep'=4,'tp'=8] {'tp'}, use_global_device_ids=true, to_apply=%region_3.0 | all-reduce | flops 8192 | bytes 32768 | tf_op jit(solution)/shard_map/psum | solution.py:84
  59.0 0.1 mul.206
  59.1 0.1 broadcast_multiply_fusion
  59.2 3.1 %multiply_add_fusion = f32[16,8,64,128]{3,2,1,0:T(8,128)S(1)} fusion(f32[16,8,64,128]{3,2,1,0:T(8,128)} %param.39, f32[16,128]{1,0:T(8,128)S(1)} %convert_multiply_fusion.5, f32[16,8,64]{2,1,0:T(8,128)S(1)} %broadcast_multiply_fusion, f32[16,8]{1,0:T(8,128)S(1)} %copy.58), kind=kLoop, calls=%fused_computation | loop fusion | flops 3145728 | bytes 8430080 | tf_op jit(solution)/shard_map/add | solution.py:105
  62.3 9.8 %fusion.68 = f32[16,1,8,64]{3,1,2,0:T(1,128)S(1)} fusion(f32[16,8,64,128]{3,2,1,0:T(8,128)S(1)} %multiply_add_fusion, f32[16,128,1,1]{1,2,3,0:T(1,128)S(1)} %bitcast.74), kind=kOutput, calls=%fused_computation.95 | convolution fusion | flops 12582912 | bytes 4235264 | tf_op jit(solution)/shard_map/shpn,sn->shp/dot_general | solution.py:108
  72.1 0.0 copy-start.2
  72.2 0.2 multiply_reduce_fusion.1
  72.4 0.1 multiply_convert_fusion
  72.5 0.1 reshape.89
  72.6 2.6 %convolution_convert_fusion.3 = bf16[16,2048]{1,0:T(8,128)(2,1)} fusion(bf16[16,512]{1,0:T(8,128)(2,1)S(1)} %reshape.89, bf16[512,2048]{1,0:T(8,128)(2,1)} %param.42), kind=kOutput, calls=%fused_computation.5 | convolution fusion | flops 33587200 | bytes 2179072 | tf_op jit(solution)/shard_map/dot_general | solution.py:113
  75.2 0.0 reduce-scatter.5.cloned.1.call-start
  75.2 0.1 copy.60
  75.3 0.1 eq.20
  75.4 0.1 fusion.42
  75.5 0.1 reduce_window_sum.11
  75.6 0.2 select_reduce_fusion.1
  75.8 0.1 reduce_sum.86
  75.9 0.1 copy.61
  76.0 0.1 convert_reduce_fusion
  76.0 52.3 %all-reduce.2.cloned.1.call-done = bf16[16,2048]{1,0:T(8,128)(2,1)} async-done(((bf16[16,2048]{1,0:T(8,128)(2,1)}), bf16[16,2048]{1,0:T(8,128)(2,1)}) %all-reduce.2.cloned.1.call-update) | async-done | bytes 65552 | tf_op jit(solution)/shard_map/psum | solution.py:114
  128.4 1.0 fusion.28
  129.4 0.3 convolution_convert_fusion.1
  129.7 10.6 %all_to_all.10 = bf16[4,2,16,2048]{3,2,1,0:T(8,128)(2,1)S(1)} all-to-all(bf16[4,2,16,2048]{3,2,1,0:T(8,128)(2,1)S(1)} %bitcast.70), channel_id=1, replica_groups=mesh['ep'=4,'tp'=8] {'ep'}, dimensions={0} | all-to-all | bytes 1048576 | tf_op jit(solution)/shard_map/all_to_all | solution.py:137
  140.3 2.0 fusion.7
  142.3 3.3 %fusion = bf16[4,2,16,2048]{3,2,0,1:T(8,128)(2,1)} fusion(bf16[2,256,2048]{2,1,0:T(8,128)(2,1)S(1)} %copy-done, bf16[2,2048,256]{2,1,0:T(8,128)(2,1)} %param.45, bf16[4,2,16,2048]{3,2,1,0:T(8,128)(2,1)S(1)} %all_to_all.10, f32[4,2,16,256]{3,2,0,1:T(8,128)S(1)} %fusion.7), kind=kOutput, calls=%fused_computation.3 | convolution fusion | flops 268894208 | bytes 5373952 | tf_op jit(solution)/shard_map/ajcf,jfd->ajcd/dot_general | solution.py:35
  145.7 0.0 reduce-scatter.3.cloned.1.call-start
  145.7 1.5 fusion.65
  147.2 2.9 %fusion.1 = bf16[1,1,16,2048]{3,2,1,0:T(8,128)(2,1)} fusion(bf16[256,2048]{1,0:T(8,128)(2,1)} %param.49, bf16[2048,256]{1,0:T(8,128)(2,1)} %param.48, f32[16,256]{1,0:T(8,128)S(1)} %fusion.65, bf16[16,2048]{1,0:T(8,128)(2,1)S(1)} %get-tuple-element.4, f32[2048]{0:T(1024)S(1)} %copy-done.6, f32[16]{0:T(128)S(1)} %add_rsqrt_fusion.1), kind=kOutput, calls=%fused_computation.6 | convolution fusion | flops 33742848 | bytes 2252864 | tf_op jit(solution)/shard_map/dot_general | solution.py:122
  150.2 0.1 select_reduce_fusion
  150.3 25.1 %reduce-scatter.5.cloned.1.call-done = bf16[4,2,16,256]{3,2,0,1:T(8,128)(2,1)} async-done(((bf16[4,2,16,2048]{3,2,0,1:T(8,128)(2,1)}), bf16[4,2,16,256]{3,2,0,1:T(8,128)(2,1)}) %reduce-scatter.5.cloned.1.call-update) | async-done | bytes 65552 | tf_op jit(solution)/shard_map/reduce_scatter | solution.py:143
  175.4 1.5 copy.64
  176.9 3.5 %all-to-all-start.1 = ((bf16[4,2,16,256]{3,2,1,0:T(8,128)(2,1)}), bf16[4,2,16,256]{3,2,1,0:T(8,128)(2,1)S(1)}, u32[]{:S(2)}, u32[]{:S(2)}) async-start(bf16[4,2,16,256]{3,2,1,0:T(8,128)(2,1)} %copy.64), calls=%async_computation.3 | async-start | bytes 131072 | tf_op jit(solution)/shard_map/all_to_all | solution.py:154
  180.4 0.6 fusion.41
  181.0 25.2 %reduce-scatter.3.cloned.1.call-done = bf16[1,1,16,256]{3,2,1,0:T(8,128)(2,1)} async-done(((bf16[1,1,16,2048]{3,2,1,0:T(8,128)(2,1)}), bf16[1,1,16,256]{3,2,1,0:T(8,128)(2,1)}) %reduce-scatter.3.cloned.1.call-update) | async-done | bytes 8208 | tf_op jit(solution)/shard_map/reduce_scatter | solution.py:146
  206.2 1.4 fusion.24
  (45 shorter events, 0.3 us)
Async XLA Ops:
  7.2 135.2 %copy-start = (bf16[2,256,2048]{2,1,0:T(8,128)(2,1)S(1)}, bf16[2,256,2048]{2,1,0:T(8,128)(2,1)}, u32[]{:S(2)}) copy-start(bf16[2,256,2048]{2,1,0:T(8,128)(2,1)} %param.46) | copy-start | bytes 6291460
  7.2 4.3 %copy-start.3 = (bf16[256,512]{1,0:T(8,128)(2,1)S(1)}, bf16[256,512]{1,0:T(8,128)(2,1)}, u32[]{:S(2)}) copy-start(bf16[256,512]{1,0:T(8,128)(2,1)} %param.32) | copy-start | bytes 786436
  7.2 20.1 %copy-start.14 = (f32[8]{0:T(128)S(1)}, f32[8]{0:T(128)}, u32[]{:S(2)}) copy-start(f32[8]{0:T(128)} %param.35) | copy-start | bytes 100
  7.2 20.1 %copy-start.13 = (f32[16,8]{0,1:T(8,128)S(1)}, f32[16,8]{0,1:T(8,128)}, u32[]{:S(2)}) copy-start(f32[16,8]{0,1:T(8,128)} %param.36) | copy-start | bytes 1540
  7.2 20.1 %copy-start.15 = (f32[8]{0:T(128)S(1)}, f32[8]{0:T(128)}, u32[]{:S(2)}) copy-start(f32[8]{0:T(128)} %param.34) | copy-start | bytes 100
  7.2 20.1 %copy-start.12 = (bf16[2048,8]{0,1:T(8,128)(2,1)S(1)}, bf16[2048,8]{0,1:T(8,128)(2,1)}, u32[]{:S(2)}) copy-start(bf16[2048,8]{0,1:T(8,128)(2,1)} %param.31) | copy-start | bytes 98308
  7.2 121.1 %all-reduce.2.cloned.1.call-start = ((), (), s32[]{:S(2)}) async-start(), calls=%async_computation.4 | async-start | bytes 131072 | tf_op jit(solution)/shard_map/psum | solution.py:114
  9.3 20.2 %copy-start.8 = (bf16[4,512]{1,0:T(4,128)(2,1)S(1)}, bf16[4,512]{1,0:T(4,128)(2,1)}, u32[]{:S(2)}) copy-start(bf16[4,512]{1,0:T(4,128)(2,1)} %param.37) | copy-start | bytes 12292
  9.4 20.2 %copy-start.5 = (bf16[16,3,512]{2,0,1:T(8,128)(2,1)S(1)}, bf16[16,3,512]{2,0,1:T(8,128)(2,1)}, u32[]{:S(2)}) copy-start(bf16[16,3,512]{2,0,1:T(8,128)(2,1)} %param.38) | copy-start | bytes 147460
  11.3 18.4 %copy-start.4 = (bf16[256,512]{1,0:T(8,128)(2,1)S(1)}, bf16[256,512]{1,0:T(8,128)(2,1)}, u32[]{:S(2)}) copy-start(bf16[256,512]{1,0:T(8,128)(2,1)} %param.33) | copy-start | bytes 786436
  11.3 47.7 %copy-start.9 = (f32[512]{0:T(512)S(1)}, f32[512]{0:T(512)}, u32[]{:S(2)}) copy-start(f32[512]{0:T(512)} %param.41) | copy-start | bytes 6148
  62.3 9.8 %copy-start.1 = (f32[16,8,64,128]{3,2,1,0:T(8,128)}, f32[16,8,64,128]{3,2,1,0:T(8,128)S(1)}, u32[]{:S(2)}) copy-start(f32[16,8,64,128]{3,2,1,0:T(8,128)S(1)} %multiply_add_fusion) | copy-start | bytes 12582916
  62.3 9.9 %copy-start.11 = (f32[8]{0:T(128)S(1)}, f32[8]{0:T(128)}, u32[]{:S(2)}) copy-start(f32[8]{0:T(128)} %param.40) | copy-start | bytes 100
  72.1 3.1 %copy-start.7 = (s32[16,4]{0,1:T(4,128)S(1)}, s32[16,4]{0,1:T(4,128)}, u32[]{:S(2)}) copy-start(s32[16,4]{0,1:T(4,128)} %param.26) | copy-start | bytes 772
  72.1 56.2 %copy-start.2 = (bf16[16,2048]{1,0:T(8,128)(2,1)S(1)}, bf16[16,2048]{1,0:T(8,128)(2,1)}, u32[]{:S(2)}) copy-start(bf16[16,2048]{1,0:T(8,128)(2,1)} %param.25) | copy-start | bytes 196612
  72.2 57.2 %copy-start.6 = (f32[2048]{0:T(1024)S(1)}, f32[2048]{0:T(1024)}, u32[]{:S(2)}) copy-start(f32[2048]{0:T(1024)} %param.43) | copy-start | bytes 24580
  75.2 100.2 %reduce-scatter.5.cloned.1.call-start = ((), (), s32[]{:S(2)}) async-start(), calls=%async_computation.6 | async-start | bytes 589824 | tf_op jit(solution)/shard_map/reduce_scatter | solution.py:143
  145.6 4.6 %copy-start.10 = (f32[16,4]{0,1:T(4,128)S(1)}, f32[16,4]{0,1:T(4,128)}, u32[]{:S(2)}) copy-start(f32[16,4]{0,1:T(4,128)} %param.27) | copy-start | bytes 772
  145.7 60.5 %reduce-scatter.3.cloned.1.call-start = ((), (), s32[]{:S(2)}) async-start(), calls=%async_computation.5 | async-start | bytes 73728 | tf_op jit(solution)/shard_map/reduce_scatter | solution.py:146
  176.9 29.3 %all-to-all-start.1 = ((bf16[4,2,16,256]{3,2,1,0:T(8,128)(2,1)}), bf16[4,2,16,256]{3,2,1,0:T(8,128)(2,1)S(1)}, u32[]{:S(2)}, u32[]{:S(2)}) async-start(bf16[4,2,16,256]{3,2,1,0:T(8,128)(2,1)} %copy.64), calls=%async_computation.3 | async-start | bytes 131072 | tf_op jit(solution)/shard_map/all_to_all | solution.py:154
Sparse Core Ops, SparseCore 0:
  75.3 53.0 all-reduce.1
  145.8 29.5 reduce-scatter.4
  177.6 28.4 reduce-scatter.2
